TPU v7x, 32 devices: a whole 2x2x4 slice. The times are simulated.
32 devices in a mesh: sp: 4 (over z), tp: 8 (over y, x, core).
Axes of the slice: x: 2, y: 2, z: 4, core: 2. Of those that a mesh axis runs over, the one named last changes fastest.
Arguments:
- target: bfloat16 [512, 2048], P('sp'), may hold values from -6 to 6
- source: bfloat16 [1024, 2048], P(('sp', 'tp')), may hold values from -6 to 6
- cotangent: bfloat16 [512, 2048], P('sp'), may hold values from -6 to 6
- target_gain: float32 [2048], replicated, may hold values from 0.1 to 1.9
- source_gain: float32 [2048], replicated, may hold values from 0.1 to 1.9
- query_weight: bfloat16 [2048, 8192], P(None, 'tp'), may hold values from -4 to 4
- key_weight: bfloat16 [2048, 2048], P(None, 'tp'), may hold values from -1 to 1
- value_projection_weight: bfloat16 [2048, 2048], P(None, 'tp'), may hold values from -0.125 to 0.125
- output_weight: bfloat16 [8192, 2048], P('tp'), may hold values from -0.0625 to 0.0625
Outputs:
- target_grad: float32 [512, 2048], P(('sp', 'tp'))
- source_grad: float32 [1024, 2048], P(('sp', 'tp'))
- key_weight_grad: float32 [2048, 2048], P(None, 'tp')
All inputs are finite; a program needn't handle non-finite values.
Results may differ from a plain program's by a relative error of at most 0.018.
The roundings to bfloat16 on the way count: a program that leaves them out, or rounds other values in their place, can miss the bound.
Values may be sent and summed in bfloat16 or wider, within the bound.
A program may use at most 64 MiB of HBM per device.

v0:
```python
import jax
import jax.numpy as jnp
from jax import lax
from jax.sharding import PartitionSpec as P

HEAD_SIZE = 256


EPSILON = 1e-05


def as_sent(array):

    def short(part):
        return part.astype(jnp.bfloat16) if part.dtype == jnp.float32 else part

    return jax.tree.map(short, array)


def partner_2(value, axis, bit):
    mask = 2**bit
    pairs = [(source, source ^ mask) for source in range(lax.axis_size(axis))]
    return lax.ppermute(value, axis, pairs)


def combined_all(value, axis, join):
    pieces = jax.tree.map(lambda part: lax.all_gather(part, axis), value)
    head = jax.tree.map(lambda part: part[0], pieces)
    tail = jax.tree.map(lambda part: part[1:], pieces)
    running, _ = lax.scan(lambda running, piece: (join(running, piece), None), head, tail)
    return running


def norm_rows(rows):
    values = rows.astype(jnp.float32)
    centred = values - jnp.mean(values, axis=-1, keepdims=True)
    inverse = lax.rsqrt(jnp.mean(centred * centred, axis=-1, keepdims=True) + EPSILON)
    return (centred * inverse, inverse)


def norm_back(scaled, inverse, gain, upstream):
    weighted = upstream * gain
    spread = jnp.mean(weighted * scaled, axis=-1, keepdims=True)
    return inverse * (weighted - jnp.mean(weighted, axis=-1, keepdims=True) - scaled * spread)


def times_transposed(left, right):
    return lax.dot_general(
        left, right, (((1,), (1,)), ((), ())), preferred_element_type=jnp.float32
    )


def split_heads(flat):
    return flat.reshape(flat.shape[0], flat.shape[1] // HEAD_SIZE, HEAD_SIZE)


def head_scores(queries, key_rows):
    return jnp.einsum(
        "rhd,sd->hrs", queries, key_rows, preferred_element_type=jnp.float32
    ) * HEAD_SIZE ** (-0.5)


def block_statistics(queries, out_grads, key_rows, value_rows):
    scores = head_scores(queries, key_rows)
    highest = jnp.max(scores, axis=2)
    weights = jnp.exp(scores - highest[:, :, None])
    products = jnp.einsum("rhd,sd->hrs", out_grads, value_rows, preferred_element_type=jnp.float32)
    return (highest, jnp.sum(weights, axis=2), jnp.sum(weights * products, axis=2))


def combine_statistics(former, latter):
    highest = jnp.maximum(former[0], latter[0])
    early_scale = jnp.exp(former[0] - highest)
    late_scale = jnp.exp(latter[0] - highest)
    return (
        highest,
        former[1] * early_scale + latter[1] * late_scale,
        former[2] * early_scale + latter[2] * late_scale,
    )


def score_grads(queries, out_grads, key_rows, value_rows, log_total, drifts):
    scores = head_scores(queries, key_rows)
    softmax_weights = jnp.exp(scores - log_total[:, :, None])
    products = jnp.einsum("rhd,sd->hrs", out_grads, value_rows, preferred_element_type=jnp.float32)
    slopes = (softmax_weights * (products - drifts[:, :, None]) * HEAD_SIZE ** (-0.5)).astype(
        jnp.bfloat16
    )
    return (softmax_weights.astype(jnp.bfloat16), slopes)


def join_heads(stacked):
    position = lax.axis_index("tp")
    part_cols = stacked.shape[2]
    bit_level = 0
    while part_cols < HEAD_SIZE:
        partner = jax.tree.map(
            lambda part, own: part.astype(own.dtype),
            partner_2(as_sent(stacked), "tp", bit_level),
            stacked,
        )
        upper_half = position >> bit_level & 1
        stacked = jnp.where(
            upper_half == 0,
            jnp.concatenate((stacked, partner), 2),
            jnp.concatenate((partner, stacked), 2),
        )
        part_cols = part_cols * 2
        bit_level = bit_level + 1
    return stacked


def split_sums(stacked, part_cols):
    position = lax.axis_index("tp")
    bit_count = (HEAD_SIZE // part_cols).bit_length() - 1
    for bit_level in reversed(range(bit_count)):
        half_cols = stacked.shape[2] // 2
        lower_half = stacked[:, :, :half_cols]
        upper_cols = stacked[:, :, half_cols:]
        upper_half = position >> bit_level & 1
        kept_half = jnp.where(upper_half == 0, lower_half, upper_cols)
        sent_half = jnp.where(upper_half == 0, upper_cols, lower_half)
        stacked = kept_half + partner_2(sent_half, "tp", bit_level)
    return stacked


def on_device(
    target,
    source,
    cotangent,
    target_gain,
    source_gain,
    query_weight,
    key_weight,
    value_projection_weight,
    output_weight,
):
    part_cols = key_weight.shape[1]
    src_scaled, src_inverse = norm_rows(source)
    src_normed = (src_scaled * source_gain).astype(jnp.bfloat16)
    tgt_scaled, tgt_inverse = norm_rows(target)
    tgt_normed = (tgt_scaled * target_gain).astype(jnp.bfloat16)
    block_rows = lax.all_gather(src_normed, "tp", axis=0, tiled=True)
    key_portion = jnp.dot(block_rows, key_weight, preferred_element_type=jnp.float32).astype(
        jnp.bfloat16
    )
    value_part = jnp.dot(
        block_rows, value_projection_weight, preferred_element_type=jnp.float32
    ).astype(jnp.bfloat16)
    parted = jnp.stack((key_portion, value_part))
    queries = split_heads(
        jnp.dot(tgt_normed, query_weight, preferred_element_type=jnp.float32).astype(jnp.bfloat16)
    )
    out_grads = split_heads(times_transposed(cotangent, output_weight).astype(jnp.bfloat16))
    head_count = queries.shape[1]
    own_rows = queries.shape[0]
    own_keys = join_heads(parted)
    all_queries, all_grads = (
        lax.all_gather(queries, "sp", axis=0, tiled=True),
        lax.all_gather(out_grads, "sp", axis=0, tiled=True),
    )
    partial_value = block_statistics(all_queries, all_grads, own_keys[0], own_keys[1])
    highest, totals, weighted = combined_all(partial_value, "sp", combine_statistics)
    log_total = highest + jnp.log(totals)
    drifts = weighted / totals
    attention, slopes = score_grads(
        all_queries, all_grads, own_keys[0], own_keys[1], log_total, drifts
    )
    key_gradient_rows = jnp.einsum(
        "hrs,rhd->sd", slopes, all_queries, preferred_element_type=jnp.float32
    )
    value_gradient_rows = jnp.einsum(
        "hrs,rhd->sd", attention, all_grads, preferred_element_type=jnp.float32
    )
    row_start = lax.axis_index("sp") * own_rows
    own_log = lax.dynamic_slice_in_dim(log_total, row_start, own_rows, 1)
    own_drifts = lax.dynamic_slice_in_dim(drifts, row_start, own_rows, 1)
    pieces = lax.all_gather(own_keys, "sp", axis=1, tiled=True)
    unused, slopes = score_grads(queries, out_grads, pieces[0], pieces[1], own_log, own_drifts)
    query_grads = jnp.einsum("hrs,sd->rhd", slopes, pieces[0], preferred_element_type=jnp.float32)
    summed = split_sums(jnp.stack((key_gradient_rows, value_gradient_rows)), part_cols)
    key_flattened = summed[0].astype(jnp.bfloat16)
    value_flattened = summed[1].astype(jnp.bfloat16)
    weight_part = lax.dot_general(
        block_rows, key_flattened, (((0,), (0,)), ((), ())), preferred_element_type=jnp.float32
    )
    key_weight_grad = lax.psum(weight_part.astype(jnp.bfloat16), "sp").astype(jnp.float32)
    source_upstream = lax.psum_scatter(
        (
            times_transposed(key_flattened, key_weight)
            + times_transposed(value_flattened, value_projection_weight)
        ).astype(jnp.bfloat16),
        "tp",
        scatter_dimension=0,
        tiled=True,
    ).astype(jnp.float32)
    source_grad = norm_back(src_scaled, src_inverse, source_gain, source_upstream)
    query_flat = query_grads.astype(jnp.bfloat16).reshape(own_rows, head_count * HEAD_SIZE)
    out_rows = own_rows // lax.axis_size("tp")
    out_start = lax.axis_index("tp") * out_rows
    target_upstream = lax.psum_scatter(
        times_transposed(query_flat, query_weight), "tp", scatter_dimension=0, tiled=True
    )
    slice_scaled = lax.dynamic_slice_in_dim(tgt_scaled, out_start, out_rows, 0)
    slice_inverse = lax.dynamic_slice_in_dim(tgt_inverse, out_start, out_rows, 0)
    slice_cotangent = lax.dynamic_slice_in_dim(cotangent, out_start, out_rows, 0)
    target_grad = slice_cotangent.astype(jnp.float32) + norm_back(
        slice_scaled, slice_inverse, target_gain, target_upstream
    )
    return (target_grad, source_grad, key_weight_grad)


def solution(mesh):
    return jax.shard_map(
        on_device,
        mesh=mesh,
        in_specs=(
            P("sp", None),
            P(("sp", "tp"), None),
            P("sp", None),
            P(),
            P(),
            P(None, "tp"),
            P(None, "tp"),
            P(None, "tp"),
            P("tp", None),
        ),
        out_specs=(P(("sp", "tp"), None), P(("sp", "tp"), None), P(None, "tp")),
        check_vma=False,
    )
```

profile of v0, /device:TPU:0, one launch (start us, length us, event | category | flops | bytes accessed | tf_op | source)
XLA Modules:
  0.0 308.4 jit_solution(17943720126214287300)
XLA Ops:
  7.2 0.0 all-gather.11.cloned.1.call-start
  7.2 1.1 convert_reduce_fusion.1
  8.3 1.1 fusion.46
  9.5 1.7 fusion.42
  11.2 0.0 all-gather.15.cloned.1.call-start
  11.2 1.2 convert_reduce_fusion
  12.4 1.3 fusion.22
  13.8 3.2 %convolution_convert_fusion.2 = bf16[128,1024]{1,0:T(8,128)(2,1)S(1)} fusion(bf16[2048,1024]{1,0:T(8,128)(2,1)} %param.16, f32[2048]{0:T(1024)} %param.14, bf16[128,2048]{1,0:T(8,128)(2,1)} %param.11, f32[128]{0:T(128)S(1)} %add_rsqrt_fusion.1, f32[128]{0:T(128)S(1)} %broadcast_multiply_fusion.5), kind=kOutput, calls=%fused_computation.38 | convolution fusion | flops 538312704 | bytes 4989952 | tf_op jit(solution)/shard_map/dot_general | solution.py:152
  17.0 0.7 copy-done.8
  17.7 0.7 copy.30
  18.4 0.0 all-gather.17.cloned.1.call-start
  18.5 3.7 %convolution_convert_fusion.1 = bf16[128,1024]{1,0:T(8,128)(2,1)S(1)} fusion(bf16[128,2048]{1,0:T(8,128)(2,1)S(1)} %copy-done.9, bf16[1024,2048]{1,0:T(8,128)(2,1)} %param.19), kind=kOutput, calls=%fused_computation.37 | convolution fusion | flops 537001984 | bytes 4980736 | tf_op jit(solution)/shard_map/dot_general | solution.py:48
  22.2 0.7 copy-done.6
  22.9 0.7 copy.29
  23.7 0.0 all-gather.13.cloned.1.call-start
  23.7 13.7 %all-gather.11.cloned.1.call-done = bf16[256,2048]{1,0:T(8,128)(2,1)} async-done(((bf16[32,2048]{1,0:T(8,128)(2,1)}), bf16[256,2048]{1,0:T(8,128)(2,1)}) %all-gather.11.cloned.1.call-update) | async-done | bytes 1048592 | tf_op jit(solution)/shard_map/all_gather | solution.py:143
  37.4 1.7 convolution_convert_fusion.4
  39.2 0.4 convolution_convert_fusion.3
  39.7 27.9 %all-gather.15.cloned.1.call-done = bf16[512,4,256]{2,0,1:T(8,128)(2,1)} async-done(((bf16[128,4,256]{2,0,1:T(8,128)(2,1)}), bf16[512,4,256]{2,0,1:T(8,128)(2,1)}) %all-gather.15.cloned.1.call-update) | async-done | bytes 1048592 | tf_op jit(solution)/shard_map/all_gather | solution.py:159
  67.6 1.7 bitcast_reduce_fusion
  69.3 27.8 %all-gather.17.cloned.1.call-done = bf16[512,4,256]{2,0,1:T(8,128)(2,1)} async-done(((bf16[128,4,256]{2,0,1:T(8,128)(2,1)}), bf16[512,4,256]{2,0,1:T(8,128)(2,1)}) %all-gather.17.cloned.1.call-update) | async-done | bytes 1048592 | tf_op jit(solution)/shard_map/all_gather | solution.py:160
  97.1 3.1 fusion.7
  100.2 13.1 %all-gather.5 = f32[4,4,512]{2,1,0:T(4,128)S(1)} all-gather(f32[1,4,512]{2,1,0:T(4,128)S(1)} %bitcast.163), channel_id=4, replica_groups=mesh['sp'=4,'tp'=8] {'sp'}, dimensions={0}, use_global_device_ids=true | all-gather | bytes 40960 | tf_op jit(solution)/shard_map/all_gather | solution.py:27
  113.3 13.1 %all-gather.4 = f32[4,4,512]{2,1,0:T(4,128)S(1)} all-gather(f32[1,4,512]{2,1,0:T(4,128)S(1)} %bitcast.162), channel_id=3, replica_groups=mesh['sp'=4,'tp'=8] {'sp'}, dimensions={0}, use_global_device_ids=true | all-gather | bytes 40960 | tf_op jit(solution)/shard_map/all_gather | solution.py:27
  126.5 13.1 %all-gather.3 = f32[4,4,512]{2,1,0:T(4,128)S(1)} all-gather(f32[1,4,512]{2,1,0:T(4,128)S(1)} %bitcast.161), channel_id=2, replica_groups=mesh['sp'=4,'tp'=8] {'sp'}, dimensions={0}, use_global_device_ids=true | all-gather | bytes 40960 | tf_op jit(solution)/shard_map/all_gather | solution.py:27
  139.6 0.7 pad_maximum_fusion
  140.4 0.0 all-reduce.2.cloned.1.call-start
  140.4 0.3 while.14
  140.7 2.5 fusion.20
  143.3 1.5 convolution_convert_fusion
  144.8 0.0 reduce-scatter.5.cloned.1.call-start
  144.8 1.8 fusion.55
  146.6 4.6 %fusion.3 = bf16[256,2048]{1,0:T(8,128)(2,1)} fusion(f32[256,2048]{1,0:T(8,128)} %fusion.55, bf16[2048,256]{1,0:T(8,128)(2,1)} %param.18, bf16[512,4,256]{2,0,1:T(8,128)(2,1)} %all-gather.17.cloned.1.call-done, f32[256,512,4]{1,0,2:T(8,128)S(1)} %get-tuple-element.70, f32[4,512]{1,0:T(4,128)S(1)} %get-tuple-element.67), kind=kOutput, calls=%fused_computation.9 | convolution fusion | flops 539033600 | bytes 7348224 | tf_op jit(solution)/shard_map/dot_general | solution.py:48
  151.2 0.0 reduce-scatter.3.cloned.1.call-start
  151.3 16.6 %all-gather.13.cloned.1.call-done = bf16[2,1024,256]{2,1,0:T(8,128)(2,1)} async-done(((bf16[2,256,256]{2,1,0:T(8,128)(2,1)}), bf16[2,1024,256]{2,1,0:T(8,128)(2,1)}) %all-gather.13.cloned.1.call-update) | async-done | bytes 1048592 | tf_op jit(solution)/shard_map/all_gather | solution.py:178
  167.9 1.6 fusion.36
  169.5 2.9 fusion.19
  172.4 4.8 %fusion.54 = f32[128,2048]{1,0:T(8,128)} fusion(bf16[128,1024]{0,1:T(8,128)(2,1)} %bitcast.160, bf16[2048,1024]{1,0:T(8,128)(2,1)} %param.16), kind=kOutput, calls=%fused_computation.98 | convolution fusion | flops 536870912 | bytes 5505024 | tf_op jit(solution)/shard_map/dot_general | solution.py:48
  177.2 0.1 dynamic-slice.3
  177.3 0.3 fusion.17
  177.7 43.8 %all-reduce.2.cloned.1.call-done = bf16[2048,256]{1,0:T(8,128)(2,1)} async-done(((bf16[2048,256]{1,0:T(8,128)(2,1)}), bf16[2048,256]{1,0:T(8,128)(2,1)}) %all-reduce.2.cloned.1.call-update) | async-done | bytes 1048592 | tf_op jit(solution)/shard_map/psum | solution.py:187
  221.4 2.7 convert_element_type.79
  224.1 35.6 %reduce-scatter.5.cloned.1.call-done = bf16[32,2048]{1,0:T(8,128)(2,1)} async-done(((bf16[256,2048]{1,0:T(8,128)(2,1)}), bf16[32,2048]{1,0:T(8,128)(2,1)}) %reduce-scatter.5.cloned.1.call-update) | async-done | bytes 131088 | tf_op jit(solution)/shard_map/reduce_scatter | solution.py:188
  259.7 1.1 fusion.47
  260.9 1.7 fusion.45
  262.6 36.3 %reduce-scatter.3.cloned.1.call-done = f32[16,2048]{1,0:T(8,128)} async-done(((f32[128,2048]{1,0:T(8,128)}), f32[16,2048]{1,0:T(8,128)}) %reduce-scatter.3.cloned.1.call-update) | async-done | bytes 131088 | tf_op jit(solution)/shard_map/reduce_scatter | solution.py:201
  298.9 1.0 multiply_reduce_fusion.1
  299.9 1.7 multiply_add_fusion
  (53 shorter events, 0.4 us)
Async XLA Ops:
  7.2 30.3 %copy-start = (bf16[2048,256]{1,0:T(8,128)(2,1)S(1)}, bf16[2048,256]{1,0:T(8,128)(2,1)}, u32[]{:S(2)}) copy-start(bf16[2048,256]{1,0:T(8,128)(2,1)} %param.17) | copy-start | bytes 3145732
  7.2 30.2 %all-gather.11.cloned.1.call-start = ((), (), s32[]{:S(2)}) async-start(), calls=%async_computation.2 | async-start | bytes 1179648 | tf_op jit(solution)/shard_map/all_gather | solution.py:143
  11.2 56.4 %all-gather.15.cloned.1.call-start = ((), (), s32[]{:S(2)}) async-start(), calls=%async_computation.4 | async-start | bytes 1310720 | tf_op jit(solution)/shard_map/all_gather | solution.py:159
  13.8 4.7 %copy-start.9 = (bf16[128,2048]{1,0:T(8,128)(2,1)S(1)}, bf16[128,2048]{1,0:T(8,128)(2,1)}, u32[]{:S(2)}) copy-start(bf16[128,2048]{1,0:T(8,128)(2,1)} %param.13) | copy-start | bytes 1572868
  17.0 0.7 copy-start.8
  18.4 78.7 %all-gather.17.cloned.1.call-start = ((), (), s32[]{:S(2)}) async-start(), calls=%async_computation.5 | async-start | bytes 1310720 | tf_op jit(solution)/shard_map/all_gather | solution.py:160
  22.2 0.7 copy-start.6
  22.2 17.0 %copy-start.4 = (bf16[2048,256]{1,0:T(8,128)(2,1)S(1)}, bf16[2048,256]{1,0:T(8,128)(2,1)}, u32[]{:S(2)}) copy-start(bf16[2048,256]{1,0:T(8,128)(2,1)} %param.18) | copy-start | bytes 3145732
  23.7 144.2 %all-gather.13.cloned.1.call-start = ((), (), s32[]{:S(2)}) async-start(), calls=%async_computation.3 | async-start | bytes 1310720 | tf_op jit(solution)/shard_map/all_gather | solution.py:178
  37.4 1.8 copy-start.1
  140.4 81.1 %all-reduce.2.cloned.1.call-start = ((), (), s32[]{:S(2)}) async-start(), calls=%async_computation.8 | async-start | bytes 2097152 | tf_op jit(solution)/shard_map/psum | solution.py:187
  140.7 2.6 copy-start.2
  144.8 115.0 %reduce-scatter.5.cloned.1.call-start = ((), (), s32[]{:S(2)}) async-start(), calls=%async_computation.7 | async-start | bytes 1179648 | tf_op jit(solution)/shard_map/reduce_scatter | solution.py:188
  151.2 18.2 %copy-start.7 = (bf16[128,1024]{1,0:T(8,128)(2,1)S(1)}, bf16[128,1024]{1,0:T(8,128)(2,1)}, u32[]{:S(2)}) copy-start(bf16[128,1024]{1,0:T(8,128)(2,1)} %copy-done.6) | copy-start | bytes 786436
  151.2 147.6 %reduce-scatter.3.cloned.1.call-start = ((), (), s32[]{:S(2)}) async-start(), calls=%async_computation.6 | async-start | bytes 1179648 | tf_op jit(solution)/shard_map/reduce_scatter | solution.py:201
  172.4 5.0 %copy-start.3 = (bf16[128,2048]{1,0:T(8,128)(2,1)S(1)}, bf16[128,2048]{1,0:T(8,128)(2,1)}, u32[]{:S(2)}) copy-start(bf16[128,2048]{1,0:T(8,128)(2,1)} %param.11) | copy-start | bytes 1572868
  177.3 82.4 %copy-start.5 = (bf16[32,2048]{1,0:T(8,128)(2,1)S(1)}, bf16[32,2048]{1,0:T(8,128)(2,1)}, u32[]{:S(2)}) copy-start(bf16[32,2048]{1,0:T(8,128)(2,1)} %param.12) | copy-start | bytes 393220
  177.3 82.4 %copy-start.10 = (f32[2048]{0:T(1024)S(1)}, f32[2048]{0:T(1024)}, u32[]{:S(2)}) copy-start(f32[2048]{0:T(1024)} %param.15) | copy-start | bytes 24580
  177.6 121.2 %copy-start.11 = (f32[2048]{0:T(1024)S(1)}, f32[2048]{0:T(1024)}, u32[]{:S(2)}) copy-start(f32[2048]{0:T(1024)} %param.14) | copy-start | bytes 24580
Sparse Core Ops, SparseCore 0:
  11.3 26.0 all-gather.10
  39.6 27.9 all-gather.14
  69.7 27.3 all-gather.16
  140.5 27.3 all-gather.12
  170.1 51.2 all-reduce.1
  224.4 35.2 reduce-scatter.4
  262.9 35.9 reduce-scatter.2
where the time goes:
time: 309 us; the launch traced here: 308 us
  waiting for transfers between devices  202 us (65%)
  blocking collectives  39.4 us (13%)
  matrix products  33.6 us (11%)
  other arithmetic  16 us (5%)
  between operations  14.3 us (5%)
    psum x1, waiting for transfers between devices, on_device(): lax.psum(weight_part.astype(jnp.bfloat16), 'sp').astype(jnp.float32)  43.8 us
    all_gather x3, blocking collectives, combined_all(): pieces = jax.tree.map(lambda part: lax.all_gather(part, axis), value)  39.4 us
    reduce_scatter x1, waiting for transfers between devices, on_device(): lax.psum_scatter(times_transposed(query_flat, query_weight), 'tp', scatte...  36.3 us
    reduce_scatter x1, waiting for transfers between devices, on_device(): lax.psum_scatter((times_transposed(key_flattened, key_weight) + times_tra...  35.6 us
    all_gather x1, waiting for transfers between devices, on_device(): lax.all_gather(queries, 'sp', axis=0, tiled=True)  27.9 us
    all_gather x1, waiting for transfers between devices, on_device(): lax.all_gather(out_grads, 'sp', axis=0, tiled=True)  27.8 us
    all_gather x1, waiting for transfers between devices, on_device(): pieces = lax.all_gather(own_keys, 'sp', axis=1, tiled=True)  16.6 us
    dot_general x4, matrix products, times_transposed(): lax.dot_general(left, right, (((1,), (1,)), ((), ())), preferred_element_...  15 us
  transfers between devices with their start and end apart: 7, of which 7 were waited for; matrix products, arithmetic and copies ran while one was open for 13% of the time, Pallas kernels for 0%

commit v1 on v0

--- a/solution.py
+++ b/solution.py
@@ -1,6 +1,10 @@
+import functools
+
 import jax
 import jax.numpy as jnp
 from jax import lax
+from jax.experimental import pallas as pl
+from jax.experimental.pallas import tpu as pltpu
 from jax.sharding import PartitionSpec as P
 
 HEAD_SIZE = 256
@@ -210,9 +214,548 @@
     return (target_grad, source_grad, key_weight_grad)
 
 
+MESH = pl.DeviceIdType.MESH
+TILE = 256
+BF16 = jnp.bfloat16
+F32 = jnp.float32
+
+
+def aligned(index, size):
+    return pl.ds(pl.multiple_of(index * size, size), size)
+
+
+def whole_step(
+    n_sp,
+    n_tp,
+    target_hbm,
+    source_hbm,
+    cotangent_hbm,
+    target_gain,
+    source_gain,
+    query_hbm,
+    key_hbm,
+    value_hbm,
+    output_hbm,
+    target_grad,
+    source_grad,
+    key_weight_grad,
+    tgt,
+    cot,
+    qw,
+    kw,
+    vw,
+    ow,
+    raw,
+    normed,
+    turned,
+    tgt_normed,
+    keys,
+    values,
+    queries,
+    grads,
+    slopes_s,
+    attention_s,
+    query_flat,
+    sums,
+    leaving,
+    arriving,
+    key_all,
+    value_flat,
+    up_t,
+    up_t_pair,
+    up_t_mid,
+    up_t_got,
+    up_s,
+    up_s_pair,
+    up_s_mid,
+    up_s_got,
+    load_sem,
+    gather_sem,
+    z_send,
+    spread_send,
+    forward_send,
+    sums_send,
+    sums_recv,
+    key_send,
+    key_recv,
+    pair_send,
+    pair_recv,
+    mid_send,
+    mid_recv,
+):
+    z = lax.axis_index("sp")
+    t = lax.axis_index("tp")
+    n_pair = n_tp // 2
+    chip = t // 2
+    core = t % 2
+    partner = chip * 2 + (1 - core)
+    depth = tgt.shape[1]
+    tgt_rows = tgt.shape[0]
+    src_rows = raw.shape[2]
+    block = n_tp * src_rows
+    out_rows = tgt_rows // n_tp
+    heads = qw.shape[1] // HEAD_SIZE
+    scale = HEAD_SIZE ** (-0.5)
+    tiles = depth // TILE
+
+    def load(index, src, dst):
+        return pltpu.make_async_copy(src, dst, load_sem.at[index])
+
+    load_src = load(0, source_hbm, raw.at[z, t])
+    load_tgt = load(1, target_hbm, tgt)
+    load_qw = load(2, query_hbm, qw)
+    load_cot = load(3, cotangent_hbm, cot)
+    load_ow = load(4, output_hbm, ow)
+    load_kw = load(5, key_hbm, kw)
+    load_vw = load(6, value_hbm, vw)
+    for each in (load_src, load_tgt, load_qw, load_cot, load_ow, load_kw, load_vw):
+        each.start()
+
+    mates = [(z, ((chip + k) % n_pair) * 2 + core) for k in range(1, n_pair)]
+    others = [((z + k) % n_sp, t) for k in range(1, n_sp)]
+    barrier = pltpu.get_barrier_semaphore()
+    for peer in mates + others + [(z, partner)]:
+        pl.semaphore_signal(barrier, inc=1, device_id=peer, device_id_type=MESH)
+    pl.semaphore_wait(barrier, len(mates) + len(others) + 1)
+
+    def remote(src, dst, send, recv, peer):
+        return pltpu.make_async_remote_copy(
+            src_ref=src,
+            dst_ref=dst,
+            send_sem=send,
+            recv_sem=recv,
+            device_id=peer,
+            device_id_type=MESH,
+        )
+
+    pending = []
+
+    def send(*args):
+        copy = remote(*args)
+        copy.start()
+        pending.append(copy)
+
+    def row_copy(zb, tb, sem, peer):
+        return (raw.at[zb, tb], raw.at[zb, tb], sem, gather_sem.at[zb, tb], peer)
+
+    def arrive(zb, tb):
+        remote(*row_copy(zb, tb, z_send.at[0], (z, partner))).wait_recv()
+
+    def spread(step):
+        zb = (z + step) % n_sp
+        if step:
+            arrive(zb, t)
+        for k in range(1, n_pair):
+            send(*row_copy(zb, t, spread_send.at[step, k], mates[k - 1]))
+        send(*row_copy(zb, t, spread_send.at[step, 0], (z, partner)))
+
+    def forward(step):
+        zb = (z + step) % n_sp
+        for k in range(1, n_pair):
+            tb = ((chip + k) % n_pair) * 2 + core
+            arrive(zb, tb)
+            send(*row_copy(zb, tb, forward_send.at[step, k], (z, partner)))
+
+    def source_block(step):
+        zb = (z + step) % n_sp
+        for k in range(n_pair):
+            arrive(zb, ((chip + k) % n_pair) * 2 + 1 - core)
+        gain = source_gain[...]
+
+        def norm_piece(piece, carry):
+            scaled, _ = norm_rows(raw[zb, piece])
+            normed[zb, aligned(piece, src_rows), :] = (scaled * gain).astype(BF16)
+            return carry
+
+        lax.fori_loop(0, n_tp, norm_piece, 0)
+        keys[aligned(zb, block), :] = jnp.dot(
+            normed[zb], kw[...], preferred_element_type=F32
+        ).astype(BF16)
+        values[aligned(zb, block), :] = jnp.dot(
+            normed[zb], vw[...], preferred_element_type=F32
+        ).astype(BF16)
+
+        def turn(j, carry):
+            turned[zb, aligned(j, TILE), :] = normed[zb, :, aligned(j, TILE)].T
+            return carry
+
+        lax.fori_loop(0, tiles, turn, 0)
+
+    near_first = sorted(range(1, n_sp), key=lambda k: min(k, n_sp - k))
+    load_src.wait()
+    for k in near_first:
+        send(*row_copy(z, t, z_send.at[k], others[k - 1]))
+    spread(0)
+
+    load_tgt.wait()
+    norm_step = tgt_rows // n_tp
+
+    def norm_target(piece, carry):
+        scaled, _ = norm_rows(tgt[aligned(piece, norm_step), :])
+        tgt_normed[aligned(piece, norm_step), :] = (scaled * target_gain[...]).astype(BF16)
+        return carry
+
+    lax.fori_loop(0, n_tp, norm_target, 0)
+    load_qw.wait()
+
+    def query_head(h, carry):
+        queries[aligned(h, tgt_rows), :] = jnp.dot(
+            tgt_normed[...], qw[:, aligned(h, HEAD_SIZE)], preferred_element_type=F32
+        ).astype(BF16)
+        return carry
+
+    lax.fori_loop(0, heads, query_head, 0)
+    spread(near_first[0])
+    forward(0)
+    load_cot.wait()
+    load_ow.wait()
+
+    def grad_head(h, carry):
+        grads[aligned(h, tgt_rows), :] = times_transposed(
+            cot[...], ow[aligned(h, HEAD_SIZE), :]
+        ).astype(BF16)
+        return carry
+
+    lax.fori_loop(0, heads, grad_head, 0)
+    for k in near_first[1:]:
+        spread(k)
+    load_kw.wait()
+    load_vw.wait()
+    source_block(0)
+    for k in near_first:
+        forward(k)
+        source_block(k)
+
+    def attend(h, carry):
+        rows = aligned(h, tgt_rows)
+        scores = times_transposed(queries[rows, :], keys[...]) * scale
+        highest = jnp.max(scores, axis=1, keepdims=True)
+        weights = jnp.exp(scores - highest)
+        totals = jnp.sum(weights, axis=1, keepdims=True)
+        products = times_transposed(grads[rows, :], values[...])
+        drifts = jnp.sum(weights * products, axis=1, keepdims=True) / totals
+        weights = weights * (1.0 / totals)
+        attention = weights.astype(BF16)
+        slopes = (weights * (products - drifts) * scale).astype(BF16)
+        for zb in range(n_sp):
+            slopes_s[zb, rows, :] = slopes[:, zb * block : (zb + 1) * block]
+            attention_s[zb, rows, :] = attention[:, zb * block : (zb + 1) * block]
+        query_flat[:, aligned(h, HEAD_SIZE)] = jnp.dot(
+            slopes, keys[...], preferred_element_type=F32
+        ).astype(BF16)
+        return carry
+
+    lax.fori_loop(0, heads, attend, 0)
+
+    def block_sums(zb, carry):
+        sums[zb, 0] = jnp.dot(slopes_s[zb].T, queries[...], preferred_element_type=F32)
+        sums[zb, 1] = jnp.dot(attention_s[zb].T, grads[...], preferred_element_type=F32)
+        return carry
+
+    lax.fori_loop(0, n_sp, block_sums, 0)
+
+    def sums_copy(side, to, part):
+        peer = (z + 1 if side == 0 else z - 1, t)
+        return remote(
+            leaving.at[to, part],
+            arriving.at[side, to, part],
+            sums_send.at[to, part],
+            sums_recv.at[side, to, part],
+            peer,
+        )
+
+    def has_upstream(side):
+        return z > 0 if side == 0 else z < n_sp - 1
+
+    def sums_wait(side, to, part):
+        pltpu.make_async_copy(
+            arriving.at[side, to, part],
+            arriving.at[side, to, part],
+            sums_recv.at[side, to, part],
+        ).wait()
+
+    def pass_on(side, far, part):
+        to = z + far if side == 0 else z - far
+        inside = to < n_sp if side == 0 else to >= 0
+
+        @pl.when(inside)
+        def _():
+            @pl.when(has_upstream(side))
+            def _():
+                sums_wait(side, to, part)
+                leaving[to, part] = (
+                    sums[to, part] + arriving[side, to, part].astype(F32)
+                ).astype(BF16)
+
+            @pl.when(jnp.logical_not(has_upstream(side)))
+            def _():
+                leaving[to, part] = sums[to, part].astype(BF16)
+
+            sums_copy(side, to, part).start()
+
+    def start_edges(side):
+        far = n_sp - 1
+
+        for part in range(2):
+            pass_on(side, far, part)
+
+    start_edges(0)
+    start_edges(1)
+
+    def target_up(j, carry):
+        tile = times_transposed(query_flat[...], qw[aligned(j, TILE), :]).astype(BF16)
+        for to in range(n_tp):
+            up_t[to % 2, to // 2, :, aligned(j, TILE)] = tile[
+                to * out_rows : (to + 1) * out_rows
+            ]
+        return carry
+
+    lax.fori_loop(0, tiles, target_up, 0)
+
+    def pair_copy(which, held, got):
+        return remote(
+            held.at[1 - core], got, pair_send.at[which], pair_recv.at[which], (z, partner)
+        )
+
+    def pair_sum(which, held, got, mid, landed):
+        pair_copy(which, held, got).wait_recv()
+        for k in list(range(1, n_pair)) + [0]:
+            to = (chip + k) % n_pair
+            mid[to] = (held[core, to].astype(F32) + got[to].astype(F32)).astype(BF16)
+            if k:
+                send(
+                    mid.at[to],
+                    landed.at[chip],
+                    mid_send.at[which, k],
+                    mid_recv.at[which, chip],
+                    mates[k - 1],
+                )
+
+    def last_sum(which, mid, landed):
+        total = mid[chip].astype(F32)
+        for k in range(1, n_pair):
+            came = (chip + k) % n_pair
+            remote(
+                mid.at[came],
+                landed.at[came],
+                mid_send.at[which, k],
+                mid_recv.at[which, came],
+                mates[k - 1],
+            ).wait_recv()
+            total = total + landed[came].astype(F32)
+        return total
+
+    target_pair = pair_copy(0, up_t, up_t_pair)
+    target_pair.start()
+    for far in range(n_sp - 2, 0, -1):
+        for part in range(2):
+            for side in range(2):
+                pass_on(side, far, part)
+        if far == n_sp - 2:
+            pair_sum(0, up_t, up_t_pair, up_t_mid, up_t_got)
+    for part in range(2):
+        for side in range(2):
+
+            @pl.when(has_upstream(side))
+            def _():
+                sums_wait(side, z, part)
+                sums[z, part] = sums[z, part] + arriving[side, z, part].astype(F32)
+
+        if part == 0:
+            key_all[z] = sums[z, 0].astype(BF16)
+            for k in near_first:
+                send(
+                    key_all.at[z],
+                    key_all.at[z],
+                    key_send.at[k],
+                    key_recv.at[z],
+                    others[k - 1],
+                )
+        else:
+            value_flat[...] = sums[z, 1].astype(BF16)
+
+    def source_up(j, carry):
+        tile = (
+            times_transposed(key_all[z], kw[aligned(j, TILE), :])
+            + times_transposed(value_flat[...], vw[aligned(j, TILE), :])
+        ).astype(BF16)
+        for to in range(n_tp):
+            up_s[to % 2, to // 2, :, aligned(j, TILE)] = tile[
+                to * src_rows : (to + 1) * src_rows
+            ]
+        return carry
+
+    lax.fori_loop(0, tiles, source_up, 0)
+    source_pair = pair_copy(1, up_s, up_s_pair)
+    source_pair.start()
+
+    own = pl.ds(pl.multiple_of(t * out_rows, out_rows), out_rows)
+    scaled, inverse = norm_rows(tgt[own, :])
+    target_grad[...] = cot[own, :].astype(F32) + norm_back(
+        scaled, inverse, target_gain[...], last_sum(0, up_t_mid, up_t_got)
+    )
+    pair_sum(1, up_s, up_s_pair, up_s_mid, up_s_got)
+
+    def weight_part(step):
+        zb = (z + step) % n_sp
+
+        def piece(j, carry):
+            product = jnp.dot(
+                turned[zb, aligned(j, TILE), :], key_all[zb], preferred_element_type=F32
+            )
+            if step:
+                product = product + key_weight_grad[aligned(j, TILE), :]
+            key_weight_grad[aligned(j, TILE), :] = product
+            return carry
+
+        lax.fori_loop(0, tiles, piece, 0)
+
+    weight_part(0)
+    for k in near_first:
+        zb = (z + k) % n_sp
+        remote(
+            key_all.at[zb], key_all.at[zb], key_send.at[k], key_recv.at[zb], others[k - 1]
+        ).wait_recv()
+        weight_part(k)
+
+    scaled, inverse = norm_rows(raw[z, t])
+    source_grad[...] = norm_back(
+        scaled, inverse, source_gain[...], last_sum(1, up_s_mid, up_s_got)
+    )
+    for copy in pending + [target_pair, source_pair]:
+        copy.wait_send()
+    for far in range(1, n_sp):
+        for part in range(2):
+            for side in range(2):
+                to = z + far if side == 0 else z - far
+
+                @pl.when(to < n_sp if side == 0 else to >= 0)
+                def _():
+                    sums_copy(side, to, part).wait_send()
+
+
+def on_device_any(
+    n_sp,
+    n_tp,
+    target,
+    source,
+    cotangent,
+    target_gain,
+    source_gain,
+    query_weight,
+    key_weight,
+    value_projection_weight,
+    output_weight,
+):
+    tgt_rows, depth = target.shape
+    src_rows = source.shape[0]
+    out_rows = tgt_rows // n_tp
+    if (
+        key_weight.shape[1] != HEAD_SIZE
+        or n_sp < 2
+        or n_tp < 4
+        or n_tp % 2
+        or depth % TILE
+        or tgt_rows % (16 * n_tp)
+        or src_rows % 16
+        or (src_rows * n_tp) % 128
+    ):
+        return on_device(
+            target,
+            source,
+            cotangent,
+            target_gain,
+            source_gain,
+            query_weight,
+            key_weight,
+            value_projection_weight,
+            output_weight,
+        )
+    n_pair = n_tp // 2
+    block = src_rows * n_tp
+    query_cols = query_weight.shape[1]
+    heads = query_cols // HEAD_SIZE
+    hbm = pl.BlockSpec(memory_space=pl.ANY)
+    vmem = pl.BlockSpec(memory_space=pltpu.VMEM)
+    dma = pltpu.SemaphoreType.DMA
+
+    def room(*shape, kind=BF16):
+        return pltpu.VMEM(shape, kind)
+
+    return pl.pallas_call(
+        functools.partial(whole_step, n_sp, n_tp),
+        out_shape=(
+            jax.ShapeDtypeStruct((out_rows, depth), F32),
+            jax.ShapeDtypeStruct((src_rows, depth), F32),
+            jax.ShapeDtypeStruct((depth, HEAD_SIZE), F32),
+        ),
+        in_specs=[hbm, hbm, hbm, vmem, vmem, hbm, hbm, hbm, hbm],
+        out_specs=(vmem, vmem, vmem),
+        scratch_shapes=[
+            room(tgt_rows, depth),
+            room(tgt_rows, depth),
+            room(depth, query_cols),
+            room(depth, HEAD_SIZE),
+            room(depth, HEAD_SIZE),
+            room(query_cols, depth),
+            room(n_sp, n_tp, src_rows, depth),
+            room(n_sp, block, depth),
+            room(n_sp, depth, block),
+            room(tgt_rows, depth),
+            room(n_sp * block, HEAD_SIZE),
+            room(n_sp * block, HEAD_SIZE),
+            room(heads * tgt_rows, HEAD_SIZE),
+            room(heads * tgt_rows, HEAD_SIZE),
+            room(n_sp, heads * tgt_rows, block),
+            room(n_sp, heads * tgt_rows, block),
+            room(tgt_rows, query_cols),
+            room(n_sp, 2, block, HEAD_SIZE, kind=F32),
+            room(n_sp, 2, block, HEAD_SIZE),
+            room(2, n_sp, 2, block, HEAD_SIZE),
+            room(n_sp, block, HEAD_SIZE),
+            room(block, HEAD_SIZE),
+            room(2, n_pair, out_rows, depth),
+            room(n_pair, out_rows, depth),
+            room(n_pair, out_rows, depth),
+            room(n_pair, out_rows, depth),
+            room(2, n_pair, src_rows, depth),
+            room(n_pair, src_rows, depth),
+            room(n_pair, src_rows, depth),
+            room(n_pair, src_rows, depth),
+            dma((7,)),
+            dma((n_sp, n_tp)),
+            dma((n_sp,)),
+            dma((n_sp, n_pair)),
+            dma((n_sp, n_pair)),
+            dma((n_sp, 2)),
+            dma((2, n_sp, 2)),
+            dma((n_sp,)),
+            dma((n_sp,)),
+            dma((2,)),
+            dma((2,)),
+            dma((2, n_pair)),
+            dma((2, n_pair)),
+        ],
+        compiler_params=pltpu.CompilerParams(
+            collective_id=0, has_side_effects=True, vmem_limit_bytes=64 * 1024 * 1024 - 65536
+        ),
+        name="whole_step",
+    )(
+        target,
+        source,
+        cotangent,
+        target_gain.reshape(1, depth),
+        source_gain.reshape(1, depth),
+        query_weight,
+        key_weight,
+        value_projection_weight,
+        output_weight,
+    )
+
+
 def solution(mesh):
     return jax.shard_map(
-        on_device,
+        functools.partial(on_device_any, mesh.shape["sp"], mesh.shape["tp"]),
         mesh=mesh,
         in_specs=(
             P("sp", None),

time: 309 us -> 84.3 us (0.27)
  waiting for transfers between devices: 202 us -> 0 us
  Pallas kernels: 0 us -> 77.1 us
  blocking collectives: 39.4 us -> 0 us
  matrix products: 33.6 us -> 0 us
  other arithmetic: 16 us -> 0 us
  between operations: 14.3 us -> 0.64 us
  local copies, waits for them, and re-layouts: 3.01 us -> 6.28 us
    all_gather x4 -> x0, waiting for transfers between devices: 86 us -> none  [the longest x1 27.9 us: on_device(): lax.all_gather(queries, 'sp', axis=0, tiled=True)]
    pallas_call x0 -> x1, Pallas kernels: none -> 77.1 us  [on_device_any(): pl.pallas_call(functools.partial(whole_step, n_sp, n_tp), out_shape=(jax....]
    reduce_scatter x2 -> x0, waiting for transfers between devices: 71.9 us -> none  [the longest x1 36.3 us: on_device(): lax.psum_scatter(times_transposed(query_flat, query_weight), 'tp', scatte...]
    psum x1 -> x0, waiting for transfers between devices: 43.8 us -> none  [on_device(): lax.psum(weight_part.astype(jnp.bfloat16), 'sp').astype(jnp.float32)]
    all_gather x3 -> x0, blocking collectives: 39.4 us -> none  [combined_all(): pieces = jax.tree.map(lambda part: lax.all_gather(part, axis), value)]
    dot_general x13 -> x0, matrix products: 33.6 us -> none  [the longest x4 15 us: times_transposed(): lax.dot_general(left, right, (((1,), (1,)), ((), ())), preferred_element_...]
    reduce_sum x6 -> x0, other arithmetic: 6.91 us -> none  [the longest x2 2.45 us: norm_rows(): jnp.mean(centred * centred, axis=-1, keepdims=True) + EPSILON]
    unnamed x24 -> x3, local copies, waits for them, and re-layouts: 1.46 us -> 6.28 us
  transfers between devices with their start and end apart: 7 -> 0, of which waited for: 7 -> 0; matrix products, arithmetic and copies ran while one was open for 13% -> 0% of each run, Pallas kernels for 0% -> 0%
where the time goes in v1:
time: 84.3 us; the launch traced here: 84 us
  Pallas kernels  77.1 us (91%)
  local copies, waits for them, and re-layouts  6.28 us (7%)
    pallas_call x1, Pallas kernels, on_device_any(): pl.pallas_call(functools.partial(whole_step, n_sp, n_tp), out_shape=(jax....  77.1 us
    unnamed x3, local copies, waits for them, and re-layouts  6.28 us

profile of v1, /device:TPU:0, one launch (start us, length us, event | category | flops | bytes accessed | tf_op | source)
XLA Modules:
  0.0 84.0 jit_solution(5879865912112136485)
XLA Ops:
  0.6 77.1 %whole_step.1 = (f32[16,2048]{1,0:T(8,128)}, f32[32,2048]{1,0:T(8,128)}, f32[2048,256]{1,0:T(8,128)}) custom-call(bf16[128,2048]{1,0:T(8,128)(2,1)} %target_hbm.1, bf16[32,2048]{1,0:T(8,128)(2,1)} %source_hbm.1, bf16[128,2048]{1,0:T(8,128)(2,1)} %cotangent_hbm.1, f32[1,2048]{1,0:T(1,128)} %bitcast.2, f32[1,2048]{1,0:T(1,128)} %bitcast.3, ...), custom_call_target="tpu_custom_call" | custom-call | tf_op jit(solution)/shard_map/whole_step/pallas_call | solution.py:685
  77.7 1.6 %copy.15 = f32[16,2048]{1,0:T(8,128)} copy(f32[16,2048]{1,0:T(8,128)} %get-tuple-element.6) | data formatting | bytes 262144
  79.3 1.7 %copy.16 = f32[32,2048]{1,0:T(8,128)} copy(f32[32,2048]{1,0:T(8,128)} %get-tuple-element.7) | data formatting | bytes 524288
  81.0 3.0 %copy.17 = f32[2048,256]{1,0:T(8,128)} copy(f32[2048,256]{1,0:T(8,128)} %get-tuple-element.8) | data formatting | bytes 4194304

commit v2 on v1

--- a/solution.py
+++ b/solution.py
@@ -274,6 +274,8 @@
     z_send,
     spread_send,
     forward_send,
+    half_send,
+    half_recv,
     sums_send,
     sums_recv,
     key_send,
@@ -311,7 +313,12 @@
     for each in (load_src, load_tgt, load_qw, load_cot, load_ow, load_kw, load_vw):
         each.start()
 
-    mates = [(z, ((chip + k) % n_pair) * 2 + core) for k in range(1, n_pair)]
+    square = n_pair == 4
+    if square:
+        across = [chip + 1 - 2 * (chip % 2), (chip + 2) % 4, 3 - chip]
+    else:
+        across = [(chip + k) % n_pair for k in range(1, n_pair)]
+    mates = [(z, other * 2 + core) for other in across]
     others = [((z + k) % n_sp, t) for k in range(1, n_sp)]
     barrier = pltpu.get_barrier_semaphore()
     for peer in mates + others + [(z, partner)]:
@@ -346,20 +353,38 @@
         if step:
             arrive(zb, t)
         for k in range(1, n_pair):
-            send(*row_copy(zb, t, spread_send.at[step, k], mates[k - 1]))
+            if not square or k != 3:
+                send(*row_copy(zb, t, spread_send.at[step, k], mates[k - 1]))
         send(*row_copy(zb, t, spread_send.at[step, 0], (z, partner)))
 
     def forward(step):
         zb = (z + step) % n_sp
         for k in range(1, n_pair):
-            tb = ((chip + k) % n_pair) * 2 + core
+            tb = mates[k - 1][1]
+            if square and k == 3:
+                continue
             arrive(zb, tb)
+            if square:
+                send(*half_copy(zb, tb, k - 1, half_send.at[step, k - 1], mates[2 - k]))
             send(*row_copy(zb, tb, forward_send.at[step, k], (z, partner)))
+
+    def half_copy(zb, tb, half, sem, peer):
+        part = raw.at[zb, tb, pl.ds(half * (src_rows // 2), src_rows // 2)]
+        return (part, part, sem, half_recv.at[zb, half], peer)
+
+    def far_corner(step):
+        if not square:
+            return
+        zb = (z + step) % n_sp
+        tb = mates[2][1]
+        for half in range(2):
+            remote(*half_copy(zb, tb, half, half_send.at[step, half], mates[0])).wait_recv()
+        send(*row_copy(zb, tb, forward_send.at[step, 3], (z, partner)))
 
     def source_block(step):
         zb = (z + step) % n_sp
-        for k in range(n_pair):
-            arrive(zb, ((chip + k) % n_pair) * 2 + 1 - core)
+        for other in [chip] + across:
+            arrive(zb, other * 2 + 1 - core)
         gain = source_gain[...]
 
         def norm_piece(piece, carry):
@@ -405,8 +430,8 @@
         return carry
 
     lax.fori_loop(0, heads, query_head, 0)
+    forward(0)
     spread(near_first[0])
-    forward(0)
     load_cot.wait()
     load_ow.wait()
 
@@ -421,10 +446,15 @@
         spread(k)
     load_kw.wait()
     load_vw.wait()
-    source_block(0)
-    for k in near_first:
-        forward(k)
+    far_corner(0)
+    steps = [0] + near_first
+    forward(steps[1])
+    for place, k in enumerate(steps):
         source_block(k)
+        if place + 1 < n_sp:
+            far_corner(steps[place + 1])
+        if place + 2 < n_sp:
+            forward(steps[place + 2])
 
     def attend(h, carry):
         rows = aligned(h, tgt_rows)
@@ -520,7 +550,7 @@
     def pair_sum(which, held, got, mid, landed):
         pair_copy(which, held, got).wait_recv()
         for k in list(range(1, n_pair)) + [0]:
-            to = (chip + k) % n_pair
+            to = across[k - 1] if k else chip
             mid[to] = (held[core, to].astype(F32) + got[to].astype(F32)).astype(BF16)
             if k:
                 send(
@@ -534,7 +564,7 @@
     def last_sum(which, mid, landed):
         total = mid[chip].astype(F32)
         for k in range(1, n_pair):
-            came = (chip + k) % n_pair
+            came = across[k - 1]
             remote(
                 mid.at[came],
                 landed.at[came],
@@ -632,6 +662,20 @@
                 @pl.when(to < n_sp if side == 0 else to >= 0)
                 def _():
                     sums_copy(side, to, part).wait_send()
+
+
+def hand_out(*refs):
+    sources, results, held = refs[:3], refs[3:6], refs[6:9]
+    in_sem, out_sem = refs[9:]
+    reads = [pltpu.make_async_copy(sources[i], held[i], in_sem.at[i]) for i in range(3)]
+    writes = [pltpu.make_async_copy(held[i], results[i], out_sem.at[i]) for i in range(3)]
+    for read in reads:
+        read.start()
+    for read, write in zip(reads, writes):
+        read.wait()
+        write.start()
+    for write in writes:
+        write.wait()
 
 
 def on_device_any(
@@ -682,7 +726,7 @@
     def room(*shape, kind=BF16):
         return pltpu.VMEM(shape, kind)
 
-    return pl.pallas_call(
+    results = pl.pallas_call(
         functools.partial(whole_step, n_sp, n_tp),
         out_shape=(
             jax.ShapeDtypeStruct((out_rows, depth), F32),
@@ -728,6 +772,8 @@
             dma((n_sp, n_pair)),
             dma((n_sp, n_pair)),
             dma((n_sp, 2)),
+            dma((n_sp, 2)),
+            dma((n_sp, 2)),
             dma((2, n_sp, 2)),
             dma((n_sp,)),
             dma((n_sp,)),
@@ -751,6 +797,15 @@
         value_projection_weight,
         output_weight,
     )
+    return pl.pallas_call(
+        hand_out,
+        out_shape=tuple(jax.ShapeDtypeStruct(each.shape, F32) for each in results),
+        in_specs=[hbm] * 3,
+        out_specs=(hbm,) * 3,
+        scratch_shapes=[room(*each.shape, kind=F32) for each in results]
+        + [dma((3,)), dma((3,))],
+        name="hand_out",
+    )(*results)
 
 
 def solution(mesh):

time: 84.3 us -> 81.9 us (0.972)
  local copies, waits for them, and re-layouts: 6.28 us -> 0 us
  Pallas kernels: 77.1 us -> 81 us
    unnamed x3 -> x0, local copies, waits for them, and re-layouts: 6.28 us -> none
    pallas_call x0 -> x1, Pallas kernels: none -> 3.12 us  [on_device_any(): pl.pallas_call(hand_out, out_shape=tuple((jax.ShapeDtypeStruct(each.shape...]
where the time goes in v2:
time: 81.9 us; the launch traced here: 81.6 us
  Pallas kernels  81 us (99%)
    pallas_call x1, Pallas kernels, on_device_any(): pl.pallas_call(functools.partial(whole_step, n_sp, n_tp), out_shape=(jax....  77.9 us
    pallas_call x1, Pallas kernels, on_device_any(): pl.pallas_call(hand_out, out_shape=tuple((jax.ShapeDtypeStruct(each.shape...  3.12 us

profile of v2, /device:TPU:0, one launch (start us, length us, event | category | flops | bytes accessed | tf_op | source)
XLA Modules:
  0.0 81.6 jit_solution(7768316311346300191)
XLA Ops:
  0.6 77.9 %whole_step.1 = (f32[16,2048]{1,0:T(8,128)}, f32[32,2048]{1,0:T(8,128)}, f32[2048,256]{1,0:T(8,128)}) custom-call(bf16[128,2048]{1,0:T(8,128)(2,1)} %target_hbm.1, bf16[32,2048]{1,0:T(8,128)(2,1)} %source_hbm.1, bf16[128,2048]{1,0:T(8,128)(2,1)} %cotangent_hbm.1, f32[1,2048]{1,0:T(1,128)} %bitcast.2, f32[1,2048]{1,0:T(1,128)} %bitcast.3, ...), custom_call_target="tpu_custom_call" | custom-call | tf_op jit(solution)/shard_map/whole_step/pallas_call | solution.py:729
  78.5 3.1 %hand_out.1 = (f32[16,2048]{1,0:T(8,128)}, f32[32,2048]{1,0:T(8,128)}, f32[2048,256]{1,0:T(8,128)}) custom-call(f32[16,2048]{1,0:T(8,128)} %get-tuple-element.6.refs_0_, f32[32,2048]{1,0:T(8,128)} %get-tuple-element.7.refs_1_, f32[2048,256]{1,0:T(8,128)} %get-tuple-element.8.refs_2_), custom_call_target="tpu_custom_call" | custom-call | tf_op jit(solution)/shard_map/hand_out/pallas_call | solution.py:800

commit v3 on v2

--- a/solution.py
+++ b/solution.py
@@ -319,7 +319,15 @@
     else:
         across = [(chip + k) % n_pair for k in range(1, n_pair)]
     mates = [(z, other * 2 + core) for other in across]
-    others = [((z + k) % n_sp, t) for k in range(1, n_sp)]
+    upper = z // ((n_sp + 1) // 2)
+    flipped = z * (1 - 2 * upper) + upper * (n_sp - 1)
+    zs = [z]
+    for k in range(1, n_sp):
+        both = (2 * flipped - k + 2 * n_sp) // (2 * n_sp)
+        turn_about = (k + 1) // 2 if k % 2 else -(k // 2)
+        place = flipped + both * turn_about + (1 - both) * (k - flipped)
+        zs.append(place * (1 - 2 * upper) + upper * (n_sp - 1))
+    others = [(zb, t) for zb in zs[1:]]
     barrier = pltpu.get_barrier_semaphore()
     for peer in mates + others + [(z, partner)]:
         pl.semaphore_signal(barrier, inc=1, device_id=peer, device_id_type=MESH)
@@ -349,7 +357,7 @@
         remote(*row_copy(zb, tb, z_send.at[0], (z, partner))).wait_recv()
 
     def spread(step):
-        zb = (z + step) % n_sp
+        zb = zs[step]
         if step:
             arrive(zb, t)
         for k in range(1, n_pair):
@@ -358,7 +366,7 @@
         send(*row_copy(zb, t, spread_send.at[step, 0], (z, partner)))
 
     def forward(step):
-        zb = (z + step) % n_sp
+        zb = zs[step]
         for k in range(1, n_pair):
             tb = mates[k - 1][1]
             if square and k == 3:
@@ -375,14 +383,14 @@
     def far_corner(step):
         if not square:
             return
-        zb = (z + step) % n_sp
+        zb = zs[step]
         tb = mates[2][1]
         for half in range(2):
             remote(*half_copy(zb, tb, half, half_send.at[step, half], mates[0])).wait_recv()
         send(*row_copy(zb, tb, forward_send.at[step, 3], (z, partner)))
 
     def source_block(step):
-        zb = (z + step) % n_sp
+        zb = zs[step]
         for other in [chip] + across:
             arrive(zb, other * 2 + 1 - core)
         gain = source_gain[...]
@@ -406,7 +414,7 @@
 
         lax.fori_loop(0, tiles, turn, 0)
 
-    near_first = sorted(range(1, n_sp), key=lambda k: min(k, n_sp - k))
+    near_first = range(1, n_sp)
     load_src.wait()
     for k in near_first:
         send(*row_copy(z, t, z_send.at[k], others[k - 1]))
@@ -431,7 +439,7 @@
 
     lax.fori_loop(0, heads, query_head, 0)
     forward(0)
-    spread(near_first[0])
+    spread(1)
     load_cot.wait()
     load_ow.wait()
 
@@ -442,19 +450,15 @@
         return carry
 
     lax.fori_loop(0, heads, grad_head, 0)
-    for k in near_first[1:]:
-        spread(k)
     load_kw.wait()
     load_vw.wait()
-    far_corner(0)
-    steps = [0] + near_first
-    forward(steps[1])
-    for place, k in enumerate(steps):
-        source_block(k)
-        if place + 1 < n_sp:
-            far_corner(steps[place + 1])
-        if place + 2 < n_sp:
-            forward(steps[place + 2])
+    for step in range(n_sp):
+        far_corner(step)
+        if step + 1 < n_sp:
+            forward(step + 1)
+        if step + 2 < n_sp:
+            spread(step + 2)
+        source_block(step)
 
     def attend(h, carry):
         rows = aligned(h, tgt_rows)
@@ -627,7 +631,7 @@
     pair_sum(1, up_s, up_s_pair, up_s_mid, up_s_got)
 
     def weight_part(step):
-        zb = (z + step) % n_sp
+        zb = zs[step]
 
         def piece(j, carry):
             product = jnp.dot(
@@ -642,7 +646,7 @@
 
     weight_part(0)
     for k in near_first:
-        zb = (z + k) % n_sp
+        zb = zs[k]
         remote(
             key_all.at[zb], key_all.at[zb], key_send.at[k], key_recv.at[zb], others[k - 1]
         ).wait_recv()

time: 81.9 us -> 81.3 us (level)
  no operation moved by 1% of the time
where the time goes in v3:
time: 81.3 us; the launch traced here: 81.1 us
  Pallas kernels  80.4 us (99%)
    pallas_call x1, Pallas kernels, on_device_any(): pl.pallas_call(functools.partial(whole_step, n_sp, n_tp), out_shape=(jax....  77.3 us
    pallas_call x1, Pallas kernels, on_device_any(): pl.pallas_call(hand_out, out_shape=tuple((jax.ShapeDtypeStruct(each.shape...  3.12 us

profile of v3, /device:TPU:0, one launch (start us, length us, event | category | flops | bytes accessed | tf_op | source)
XLA Modules:
  0.0 81.1 jit_solution(2381773822822746696)
XLA Ops:
  0.6 77.3 %whole_step.1 = (f32[16,2048]{1,0:T(8,128)}, f32[32,2048]{1,0:T(8,128)}, f32[2048,256]{1,0:T(8,128)}) custom-call(bf16[128,2048]{1,0:T(8,128)(2,1)} %target_hbm.1, bf16[32,2048]{1,0:T(8,128)(2,1)} %source_hbm.1, bf16[128,2048]{1,0:T(8,128)(2,1)} %cotangent_hbm.1, f32[1,2048]{1,0:T(1,128)} %bitcast.2, f32[1,2048]{1,0:T(1,128)} %bitcast.3, ...), custom_call_target="tpu_custom_call" | custom-call | tf_op jit(solution)/shard_map/whole_step/pallas_call | solution.py:733
  77.9 3.1 %hand_out.1 = (f32[16,2048]{1,0:T(8,128)}, f32[32,2048]{1,0:T(8,128)}, f32[2048,256]{1,0:T(8,128)}) custom-call(f32[16,2048]{1,0:T(8,128)} %get-tuple-element.6.refs_0_, f32[32,2048]{1,0:T(8,128)} %get-tuple-element.7.refs_1_, f32[2048,256]{1,0:T(8,128)} %get-tuple-element.8.refs_2_), custom_call_target="tpu_custom_call" | custom-call | tf_op jit(solution)/shard_map/hand_out/pallas_call | solution.py:804
